TPU v7x, 32 devices: a whole 2x2x4 slice. The times are simulated.
32 devices in a mesh: grp: 2 (over y), ep: 4 (over z), tp: 4 (over x, core).
Axes of the slice: x: 2, y: 2, z: 4, core: 2. Of those that a mesh axis runs over, the one named last changes fastest.
Arguments:
- mix_rows: bfloat16 [4096, 2048], P(('grp', 'ep', 'tp')), parts along dimension 0, may hold values from -6 to 6
- expert_rows: bfloat16 [4096, 2048], P(('grp', 'ep', 'tp')), parts along dimension 0, may hold values from -6 to 6
- mix_gain: float32 [2048], replicated, may hold values from 0.1 to 1.9
- ffn_gain: float32 [2048], replicated, may hold values from 0.1 to 1.9
- w_query: bfloat16 [2048, 512], P(None, 'tp'), may hold values from -0.125 to 0.125
- w_key: bfloat16 [2048, 512], P(None, 'tp'), may hold values from -0.125 to 0.125
- w_value: bfloat16 [2048, 1024], P(None, 'tp'), may hold values from -0.125 to 0.125
- w_lowrank: bfloat16 [2048, 32], replicated, may hold values from -0.125 to 0.125
- w_decay: bfloat16 [32, 512], replicated, may hold values from -1 to 1
- decay_bias: float32 [512], replicated, may hold values from -1.5 to 16
- decay_shift: float32 [8, 4096], P('tp', ('grp', 'ep')), parts along dimension 1, may hold values from -2 to 0
- head_gain: float32 [128], replicated, may hold values from 0.1 to 1.9
- w_output: bfloat16 [1024, 2048], P('tp'), may hold values from -0.1875 to 0.1875
- route_ids: int32 [4096, 4], P(('grp', 'ep', 'tp')), parts along dimension 0, may hold values from 0 to 15, all different within a row; in each aligned block of 128 rows (0 to 127, 128 to 255, ...) at most 64 rows name the same one
- route_weights: float32 [4096, 4], P(('grp', 'ep', 'tp')), parts along dimension 0, may hold values from 0.3 to 1.2
- w_gate: bfloat16 [16, 2048, 512], P(('ep', 'tp')), may hold values from -0.125 to 0.125
- w_lift: bfloat16 [16, 2048, 512], P(('ep', 'tp')), may hold values from -0.125 to 0.125
- w_drop: bfloat16 [16, 512, 2048], P(('ep', 'tp')), may hold values from -0.25 to 0.25
- shared_gate: bfloat16 [2048, 512], P(None, 'tp'), may hold values from -0.125 to 0.125
- shared_lift: bfloat16 [2048, 512], P(None, 'tp'), may hold values from -0.125 to 0.125
- shared_drop: bfloat16 [512, 2048], P('tp'), may hold values from -0.25 to 0.25
Outputs:
- mixed: bfloat16 [4096, 2048], P(('grp', 'ep', 'tp')), parts along dimension 0
- expert_out: bfloat16 [4096, 2048], P(('grp', 'ep', 'tp')), parts along dimension 0
There are 2 independent parts, one for each index of `grp`. A program takes and returns all parts, laid end to end along the dimension named above; an argument that names none is the same for every part. Nothing has to cross between parts.
Inputs may be any that keep to these rules, and one draw needn't show every extreme that they name: `route_ids`: each row names 4 different experts. In each aligned block of 128 rows (the rows of one device) no expert is named by more than 64 rows.
All inputs are finite; a program needn't handle non-finite values.
Results may differ from a plain program's by a relative error of at most 0.014.
Values may be sent and summed in bfloat16 or wider, within the bound.
A program may use at most 128 MiB of HBM per device.

v0:
```python
import jax
import jax.numpy as jnp
from jax import lax
from jax.sharding import PartitionSpec as P

DK = 64
DV = 128
BLOCK = 64
epsilon = 1e-05
gate_norm = 16.0
highest = lax.Precision.HIGHEST


def entering_2(value, axis, combine, identity):
    length, mine = (lax.axis_size(axis), lax.axis_index(axis))
    everything = jax.tree.map(
        lambda part, kind: lax.all_gather(part.astype(kind), axis),
        value,
        (jnp.bfloat16, jnp.bfloat16),
    )
    start = jax.tree.map(
        lambda part, zero: jnp.broadcast_to(jnp.asarray(zero, part.dtype), part.shape),
        value,
        identity,
    )

    def lap(k, before):
        reached = k < mine
        new = combine(
            before, jax.tree.map(lambda part, own: part[k].astype(own.dtype), everything, value)
        )
        return jax.tree.map(lambda a, b: jnp.where(reached, a, b), new, before)

    return lax.fori_loop(0, length, lap, start)


def layer_norm(source, gain):
    values = source.astype(jnp.float32)
    center = values - jnp.mean(values, axis=-1, keepdims=True)
    inverse = lax.rsqrt(jnp.mean(center * center, axis=-1, keepdims=True) + epsilon)
    return (center * inverse * gain).astype(jnp.bfloat16)


def stored(product):
    return lax.optimization_barrier(product.astype(jnp.bfloat16)).astype(jnp.float32)


def gla_blocks(queries, key_rows, value_rows, log_decay, state_init):
    length, heads_here, key_width = queries.shape
    value_width = value_rows.shape[-1]
    blocks = length // BLOCK
    query_blocks = queries.reshape(blocks, BLOCK, heads_here, key_width)
    key_blocks = key_rows.reshape(blocks, BLOCK, heads_here, key_width)
    value_blocks = value_rows.reshape(blocks, BLOCK, heads_here, value_width)
    within = jnp.cumsum(log_decay.reshape(blocks, BLOCK, heads_here, key_width), axis=1)
    block_total = within[:, -1]
    scaled_query = query_blocks * jnp.exp(within)
    scaled_key = key_blocks * jnp.exp(-within)
    causal = jnp.tril(jnp.ones((BLOCK, BLOCK), dtype=jnp.bool_))
    scores = jnp.einsum("nihd,njhd->nhij", scaled_query, scaled_key, precision=highest)
    scores = jnp.where(causal, scores, 0.0)
    inside = jnp.einsum("nhij,njhv->nihv", scores, value_blocks, precision=highest)
    block_added = jnp.einsum(
        "njhd,njhv->nhdv",
        key_blocks * jnp.exp(block_total[:, None] - within),
        value_blocks,
        precision=highest,
    )

    def advance(state, inputs):
        decay_sum, addition = inputs
        return (jnp.exp(decay_sum)[:, :, None] * state + addition, state)

    final_state, entering = lax.scan(advance, state_init, (block_total, block_added))
    inside = inside + jnp.einsum("nihd,nhdv->nihv", scaled_query, entering, precision=highest)
    before = jnp.cumsum(block_total, axis=0) - block_total
    carried_query = query_blocks * jnp.exp(within + before[:, None])
    return (
        inside.reshape(length, heads_here, value_width),
        final_state,
        carried_query.reshape(length, heads_here, key_width),
        jnp.sum(block_total, axis=0),
    )


def body(
    mix_rows,
    expert_rows,
    mix_gain,
    ffn_gain,
    w_query,
    w_key,
    w_value,
    w_lowrank,
    w_decay,
    decay_bias,
    decay_shift,
    head_gain,
    w_output,
    route_ids,
    route_weights,
    w_gate,
    w_lift,
    w_drop,
    shared_gate,
    shared_lift,
    shared_drop,
):
    mix_normed = layer_norm(mix_rows, mix_gain)
    local_heads = w_query.shape[1] // DK
    key_cols = local_heads * DK
    value_cols = w_value.shape[1]
    column = lax.axis_index("tp") * key_cols
    decay_cols = lax.dynamic_slice_in_dim(w_decay, column, key_cols, 1)
    bias_cols = lax.dynamic_slice_in_dim(decay_bias, column, key_cols, 0)
    shard_rows = lax.all_gather(mix_normed, "tp", axis=0, tiled=True)
    query_part = jnp.dot(shard_rows, w_query, preferred_element_type=jnp.float32)
    key_part = jnp.dot(shard_rows, w_key, preferred_element_type=jnp.float32)
    value_part = jnp.dot(shard_rows, w_value, preferred_element_type=jnp.float32)
    lowrank = jnp.dot(shard_rows, w_lowrank, preferred_element_type=jnp.float32).astype(
        jnp.bfloat16
    )
    logits = jnp.dot(lowrank, decay_cols, preferred_element_type=jnp.float32) + bias_cols
    projected = jnp.concatenate(
        [stored(query_part), stored(key_part), stored(value_part), logits], axis=1
    )
    span_rows = projected.shape[0]
    queries = projected[:, :key_cols].reshape(span_rows, local_heads, DK) * DK ** (-0.5)
    key_rows = projected[:, key_cols : 2 * key_cols].reshape(span_rows, local_heads, DK)
    value_rows = projected[:, 2 * key_cols : 2 * key_cols + value_cols].reshape(
        span_rows, local_heads, DV
    )
    log_decay = (
        jax.nn.log_sigmoid(projected[:, 2 * key_cols + value_cols :]).reshape(
            span_rows, local_heads, DK
        )
        / gate_norm
        + jnp.transpose(decay_shift)[:, :, None]
    )
    zero_state = jnp.zeros((local_heads, DK, DV), jnp.float32)
    inside, final_state, carried_query, decay_total = gla_blocks(
        queries, key_rows, value_rows, log_decay, zero_state
    )

    def chain(earlier, later):
        return (earlier[0] + later[0], jnp.exp(later[0])[:, :, None] * earlier[1] + later[1])

    carried = entering_2(
        (decay_total, final_state), "ep", chain, (jnp.zeros_like(decay_total), zero_state)
    )
    entering = carried[1]
    attended = inside + jnp.einsum("rhd,hdv->rhv", carried_query, entering, precision=highest)
    inverse = lax.rsqrt(jnp.mean(attended * attended, axis=-1, keepdims=True) + epsilon)
    head_rows = (
        (attended * inverse * head_gain).astype(jnp.bfloat16).reshape(span_rows, local_heads * DV)
    )
    mixed = lax.psum_scatter(
        jnp.dot(head_rows, w_output, preferred_element_type=jnp.float32).astype(jnp.bfloat16),
        "tp",
        scatter_dimension=0,
        tiled=True,
    )
    expert_normed = layer_norm(expert_rows, ffn_gain)
    shard_rows = lax.all_gather(expert_normed, "tp", axis=0, tiled=True)
    hidden = (
        jax.nn.silu(jnp.dot(shard_rows, shared_gate, preferred_element_type=jnp.float32))
        * jnp.dot(shard_rows, shared_lift, preferred_element_type=jnp.float32)
    ).astype(jnp.bfloat16)
    shared_sum = lax.psum_scatter(
        jnp.dot(hidden, shared_drop, preferred_element_type=jnp.float32).astype(jnp.bfloat16),
        "tp",
        scatter_dimension=0,
        tiled=True,
    ).astype(jnp.float32)
    own_tokens, top_count = route_ids.shape
    local_experts = w_gate.shape[0]
    experts = lax.axis_size("ep") * lax.axis_size("tp") * local_experts
    capacity = 2 * own_tokens * top_count // experts
    flat_routes = route_ids.reshape(-1)
    matches = (flat_routes[:, None] == jnp.arange(experts, dtype=jnp.int32)[None, :]).astype(
        jnp.int32
    )
    slot_rank = jnp.sum((jnp.cumsum(matches, axis=0) - 1) * matches, axis=1)
    slot_index = flat_routes * capacity + slot_rank
    token_index = jnp.arange(own_tokens * top_count, dtype=jnp.int32) // top_count
    slot_token = (
        jnp.full((experts * capacity,), own_tokens, jnp.int32).at[slot_index].set(token_index)
    )
    padded = jnp.concatenate(
        [expert_normed, jnp.zeros((1, expert_normed.shape[1]), jnp.bfloat16)], axis=0
    )
    outgoing = padded[slot_token].reshape(experts, capacity, -1)
    arrived = lax.all_to_all(outgoing, ("ep", "tp"), split_axis=0, concat_axis=0, tiled=True)
    arrived_shape = arrived.shape
    grouped = arrived.reshape(-1, local_experts, arrived_shape[-2], arrived_shape[-1])
    gate_part = jnp.einsum("sepd,edf->sepf", grouped, w_gate, preferred_element_type=jnp.float32)
    lift_part = jnp.einsum("sepd,edf->sepf", grouped, w_lift, preferred_element_type=jnp.float32)
    inner = (jax.nn.silu(gate_part) * lift_part).astype(jnp.bfloat16)
    result = jnp.einsum("sepf,efd->sepd", inner, w_drop, preferred_element_type=jnp.float32)
    returned = lax.all_to_all(
        result.astype(jnp.bfloat16).reshape(arrived_shape),
        ("ep", "tp"),
        split_axis=0,
        concat_axis=0,
        tiled=True,
    )
    results = returned.reshape(experts * capacity, -1)[slot_index].reshape(
        own_tokens, top_count, -1
    )
    combined = shared_sum + jnp.sum(route_weights[:, :, None] * results.astype(jnp.float32), axis=1)
    return (mixed, combined.astype(jnp.bfloat16))


def solution(mesh):
    return jax.shard_map(
        body,
        mesh=mesh,
        in_specs=(
            P(("grp", "ep", "tp"), None),
            P(("grp", "ep", "tp"), None),
            P(),
            P(),
            P(None, "tp"),
            P(None, "tp"),
            P(None, "tp"),
            P(),
            P(),
            P(),
            P("tp", ("grp", "ep")),
            P(),
            P("tp", None),
            P(("grp", "ep", "tp"), None),
            P(("grp", "ep", "tp"), None),
            P(("ep", "tp"), None, None),
            P(("ep", "tp"), None, None),
            P(("ep", "tp"), None, None),
            P(None, "tp"),
            P(None, "tp"),
            P("tp", None),
        ),
        out_specs=(P(("grp", "ep", "tp"), None), P(("grp", "ep", "tp"), None)),
        check_vma=False,
    )
```

profile of v0, /device:TPU:0, one launch (start us, length us, event | category | flops | bytes accessed | tf_op | source)
XLA Modules:
  0.0 297.1 jit_solution(844361430291442152)
XLA Ops:
  10.8 2.4 scatter_custom_fusion
  13.2 1.2 convert_reduce_fusion
  14.5 1.3 fusion.23
  15.8 1.4 fusion.25
  17.3 6.0 %gather_fusion = bf16[1024,2048]{1,0:T(8,128)(2,1)} fusion(bf16[129,2048]{1,0:T(8,128)(2,1)S(1)} %concatenate.3, s32[1024]{0:T(1024)S(1)} %fusion.54), kind=kCustom, calls=%fused_computation | custom fusion | bytes 8392704 | tf_op jit(solution)/shard_map/gather | solution.py:192
  23.3 7.6 %all-to-all-start = ((bf16[16,64,2048]{2,1,0:T(8,128)(2,1)}), bf16[16,64,2048]{2,1,0:T(8,128)(2,1)}, u32[]{:S(2)}, u32[]{:S(2)}) async-start(bf16[16,64,2048]{2,1,0:T(8,128)(2,1)} %bitcast.142), calls=%async_computation.2 | async-start | bytes 8388608 | tf_op jit(solution)/shard_map/all_to_all | solution.py:193
  34.4 42.4 %all-gather.6.cloned.1.call-done = bf16[512,2048]{1,0:T(8,128)(2,1)} async-done(((bf16[128,2048]{1,0:T(8,128)(2,1)}), bf16[512,2048]{1,0:T(8,128)(2,1)}) %all-gather.6.cloned.1.call-update) | async-done | bytes 2097168 | tf_op jit(solution)/shard_map/all_gather | solution.py:116
  76.8 2.7 fusion.38
  80.4 2.6 convolution_convert_fusion.5
  84.2 2.7 convolution_convert_fusion.4
  88.0 2.6 convolution_convert_fusion.3
  90.6 19.8 %all-gather.8.cloned.1.call-done = bf16[512,2048]{1,0:T(8,128)(2,1)} async-done(((bf16[128,2048]{1,0:T(8,128)(2,1)}), bf16[512,2048]{1,0:T(8,128)(2,1)}) %all-gather.8.cloned.1.call-update) | async-done | bytes 2097168 | tf_op jit(solution)/shard_map/all_gather | solution.py:164
  110.5 2.4 fusion.63
  112.8 5.5 %convolution_convert_fusion.1 = bf16[512,2048]{1,0:T(8,128)(2,1)} fusion(bf16[128,2048]{1,0:T(8,128)(2,1)} %param.45, bf16[512,2048]{1,0:T(8,128)(2,1)} %all-gather.8.cloned.1.call-done, bf16[2048,128]{1,0:T(8,128)(2,1)} %param.44, f32[512,128]{1,0:T(8,128)S(1)} %fusion.63), kind=kOutput, calls=%fused_computation.12 | convolution fusion | flops 538312704 | bytes 5505024 | tf_op jit(solution)/shard_map/dot_general | solution.py:170
  119.5 3.1 %exponential_multiply_fusion = (f32[8,64,2,64]{3,0,1,2:T(8,128)S(1)}, f32[8,64,2,64]{3,0,1,2:T(8,128)}, f32[8,64,2,64]{3,0,1,2:T(8,128)}, f32[8,64,2,64]{3,0,1,2:T(8,128)S(1)}) fusion(f32[8,64,2,64]{3,0,1,2:T(8,128)} %copy-done.3, f32[8,64,2,64]{3,2,1,0:T(2,128)} %reshape.186, f32[8,2,64]{2,0,1:T(8,128)S(1)} %get-tuple-element.272, ...), kind=kLoop, calls=%fused_computation.65 | loop fusion | flops 393216 | bytes 1843200 | tf_op jit(solution)/shard_map/mul | solution.py:65
  122.5 1.4 fusion.31
  123.9 6.9 %fusion.3 = f32[16,64,512]{2,1,0:T(8,128)} fusion(bf16[16,64,2048]{2,1,0:T(8,128)(2,1)} %all-to-all-done, bf16[1,2048,512]{2,1,0:T(8,128)(2,1)} %param.41), kind=kOutput, calls=%fused_computation.17 | convolution fusion | flops 2147483648 | bytes 8388608 | tf_op jit(solution)/shard_map/sepd,edf->sepf/dot_general | solution.py:197
  130.8 10.5 %convolution_convert_fusion = bf16[16,64,2048]{2,1,0:T(8,128)(2,1)} fusion(bf16[1,512,2048]{2,1,0:T(8,128)(2,1)S(1)} %copy-done, f32[16,64,512]{2,1,0:T(8,128)} %fusion.3, bf16[16,64,2048]{2,1,0:T(8,128)(2,1)} %all-to-all-done, bf16[1,2048,512]{2,1,0:T(8,128)(2,1)} %param.40), kind=kOutput, calls=%fused_computation.11 | convolution fusion | flops 4300210176 | bytes 14680064 | tf_op jit(solution)/shard_map/sepf,efd->sepd/dot_general | solution.py:199
  141.3 4.5 %all-to-all-start.1 = ((bf16[16,64,2048]{2,1,0:T(8,128)(2,1)}), bf16[16,64,2048]{2,1,0:T(8,128)(2,1)}, u32[]{:S(2)}, u32[]{:S(2)}) async-start(bf16[16,64,2048]{2,1,0:T(8,128)(2,1)} %convolution_convert_fusion), calls=%async_computation.3 | async-start | bytes 8388608 | tf_op jit(solution)/shard_map/all_to_all | solution.py:200
  145.9 13.0 %while.27 = (s32[]{:T(128)}, f32[2,64,128]{2,1,0:T(8,128)S(1)}, f32[8,2,64,128]{3,2,1,0:T(8,128)}, f32[8,2,64]{2,0,1:T(8,128)S(1)}, f32[8,2,64,128]{3,2,1,0:T(8,128)}, /*index=5*/s32[]{:T(128)}, s32[]{:T(128)}) while((s32[]{:T(128)}, f32[2,64,128]{2,1,0:T(8,128)S(1)}, f32[8,2,64,128]{3,2,1,0:T(8,128)}, f32[8,2,64]{2,0,1:T(8,128)S(1)}, ...), condition=%wide.region_4.5_spmd.clone, body=%wide.region_3.4_spmd.clone.sunk | while | flops 65539 | bytes 330848 | solution.py:74
  160.4 2.1 convolution_select_fusion
  164.4 1.2 copy.69
  166.7 1.2 exp.58
  167.9 52.2 %all-gather.2 = bf16[4,2,64]{2,1,0:T(2,128)(2,1)S(1)} all-gather(bf16[1,2,64]{2,1,0:T(2,128)(2,1)S(1)} %bitcast.152), channel_id=2, replica_groups=mesh['grp'=2,'ep'=4,'tp'=4] {'ep'}, dimensions={0}, use_global_device_ids=true | all-gather | bytes 1280 | tf_op jit(solution)/shard_map/all_gather | solution.py:17
  220.2 34.7 %all-gather.1 = bf16[8,64,128]{2,1,0:T(8,128)(2,1)S(1)} all-gather(bf16[2,64,128]{2,1,0:T(8,128)(2,1)} %convert_element_type.114), channel_id=3, replica_groups=mesh['grp'=2,'ep'=4,'tp'=4] {'ep'}, dimensions={0}, use_global_device_ids=true | all-gather | bytes 163840 | tf_op jit(solution)/shard_map/all_gather | solution.py:17
  255.4 1.7 multiply_reduce_fusion.1
  257.2 2.1 convolution_convert_fusion.2
  260.2 7.9 %gather_fusion.1 = bf16[512,2048]{1,0:T(8,128)(2,1)} fusion(bf16[1024,2048]{1,0:T(8,128)(2,1)} %bitcast.29, s32[1024]{0:T(1024)S(1)} %pad_clamp_fusion), kind=kCustom, calls=%fused_computation.1 | custom fusion | bytes 4196352 | tf_op jit(solution)/shard_map/gather | solution.py:207
  268.2 4.9 %reshape.187 = f32[128,4,2048]{2,1,0:T(4,128)} reshape(bf16[512,2048]{1,0:T(8,128)(2,1)} %gather_fusion.1) | data formatting | bytes 6291456 | tf_op jit(solution)/shard_map/convert_element_type | solution.py:210
  273.0 5.4 %multiply_reduce_fusion = f32[128,2048]{1,0:T(8,128)S(1)} fusion(f32[128,4,2048]{2,1,0:T(4,128)} %reshape.187, f32[128,4]{1,0:T(8,128)S(1)} %copy.70), kind=kLoop, calls=%fused_computation.10 | loop fusion | flops 1835008 | bytes 5244928 | tf_op jit(solution)/shard_map/reduce_sum | solution.py:210
  278.4 1.9 add_convert_fusion
  280.4 10.2 %reduce-scatter.3.cloned.1.call-done = bf16[128,2048]{1,0:T(8,128)(2,1)} async-done(((bf16[512,2048]{1,0:T(8,128)(2,1)}), bf16[128,2048]{1,0:T(8,128)(2,1)}) %reduce-scatter.3.cloned.1.call-update) | async-done | bytes 524304 | tf_op jit(solution)/shard_map/reduce_scatter | solution.py:157
  (128 shorter events, 30.3 us)
Async XLA Ops:
  7.2 123.7 %copy-start = (bf16[1,512,2048]{2,1,0:T(8,128)(2,1)S(1)}, bf16[1,512,2048]{2,1,0:T(8,128)(2,1)}, u32[]{:S(2)}) copy-start(bf16[1,512,2048]{2,1,0:T(8,128)(2,1)} %param.42) | copy-start | bytes 6291460
  17.2 6.1 %copy-start.2 = (bf16[128,2048]{1,0:T(8,128)(2,1)}, bf16[128,2048]{1,0:T(8,128)(2,1)S(1)}, u32[]{:S(2)}) copy-start(bf16[128,2048]{1,0:T(8,128)(2,1)S(1)} %fusion.25) | copy-start | bytes 1572868
  23.3 7.7 %copy-start.1 = (bf16[128,2048]{1,0:T(8,128)(2,1)S(1)}, bf16[128,2048]{1,0:T(8,128)(2,1)}, u32[]{:S(2)}) copy-start(bf16[128,2048]{1,0:T(8,128)(2,1)} %param.25) | copy-start | bytes 1572868
  23.3 8.1 %copy-start.8 = (f32[2048]{0:T(1024)S(1)}, f32[2048]{0:T(1024)}, u32[]{:S(2)}) copy-start(f32[2048]{0:T(1024)} %param.27) | copy-start | bytes 24580
  23.3 100.6 %all-to-all-start = ((bf16[16,64,2048]{2,1,0:T(8,128)(2,1)}), bf16[16,64,2048]{2,1,0:T(8,128)(2,1)}, u32[]{:S(2)}, u32[]{:S(2)}) async-start(bf16[16,64,2048]{2,1,0:T(8,128)(2,1)} %bitcast.142), calls=%async_computation.2 | async-start | bytes 8388608 | tf_op jit(solution)/shard_map/all_to_all | solution.py:193
  30.9 2.6 copy-start.9
  30.9 45.9 %copy-start.12 = (bf16[2048,32]{0,1:T(8,128)(2,1)S(1)}, bf16[2048,32]{0,1:T(8,128)(2,1)}, u32[]{:S(2)}) copy-start(bf16[2048,32]{0,1:T(8,128)(2,1)} %param.32) | copy-start | bytes 393220
  30.9 45.9 %all-gather.6.cloned.1.call-start = ((), (), s32[]{:S(2)}) async-start(), calls=%async_computation.4 | async-start | bytes 2621440 | tf_op jit(solution)/shard_map/all_gather | solution.py:116
  32.6 77.8 %all-gather.8.cloned.1.call-start = ((), (), s32[]{:S(2)}) async-start(), calls=%async_computation.6 | async-start | bytes 2621440 | tf_op jit(solution)/shard_map/all_gather | solution.py:164
  33.4 245.0 %reduce-scatter.5.cloned.1.call-start = ((), (), s32[]{:S(2)}) async-start(), calls=%async_computation.7 | async-start | bytes 2621440 | tf_op jit(solution)/shard_map/reduce_scatter | solution.py:169
  80.4 6.4 %copy-start.3 = (f32[8,64,2,64]{3,0,1,2:T(8,128)}, f32[8,64,2,64]{3,0,1,2:T(8,128)S(1)}, u32[]{:S(2)}) copy-start(f32[8,64,2,64]{3,0,1,2:T(8,128)S(1)} %fusion.34) | copy-start | bytes 786436
  118.3 0.7 slice-start
  118.3 1.1 copy-start.4
  141.3 118.9 %all-to-all-start.1 = ((bf16[16,64,2048]{2,1,0:T(8,128)(2,1)}), bf16[16,64,2048]{2,1,0:T(8,128)(2,1)}, u32[]{:S(2)}, u32[]{:S(2)}) async-start(bf16[16,64,2048]{2,1,0:T(8,128)(2,1)} %convolution_convert_fusion), calls=%async_computation.3 | async-start | bytes 8388608 | tf_op jit(solution)/shard_map/all_to_all | solution.py:200
  145.8 144.7 %reduce-scatter.3.cloned.1.call-start = ((), (), s32[]{:S(2)}) async-start(), calls=%async_computation.5 | async-start | bytes 2621440 | tf_op jit(solution)/shard_map/reduce_scatter | solution.py:157
  159.8 3.1 %copy-start.7 = (f32[8,2,64,128]{3,2,1,0:T(8,128)S(1)}, f32[8,2,64,128]{3,2,1,0:T(8,128)}, u32[]{:S(2)}) copy-start(f32[8,2,64,128]{3,2,1,0:T(8,128)} %get-tuple-element.124) | copy-start | bytes 1572868
  162.9 2.8 copy-start.5
  165.7 91.4 %copy-start.11 = (f32[128]{0:T(128)S(1)}, f32[128]{0:T(128)}, u32[]{:S(2)}) copy-start(f32[128]{0:T(128)} %param.36) | copy-start | bytes 1540
  255.4 1.9 copy-start.6
  259.4 0.7 copy-start.10
Sparse Core Ops, SparseCore 0:
  33.8 42.9 all-gather.5
  78.4 32.0 all-gather.7
  118.5 29.2 reduce-scatter.4
  259.5 30.9 reduce-scatter.2
where the time goes:
time: 299 us; the launch traced here: 297 us
  blocking collectives  86.9 us (29%)
  waiting for transfers between devices  73.2 us (24%)
  matrix products  44.2 us (15%)
  local copies, waits for them, and re-layouts  33.6 us (11%)
  other arithmetic  32.3 us (11%)
  between operations  14.2 us (5%)
  starting transfers between devices  12.3 us (4%)
    all_gather x2, blocking collectives, entering_2(): lax.all_gather(part.astype(kind), axis)  86.9 us
    all_gather x1, waiting for transfers between devices, body(): shard_rows = lax.all_gather(mix_normed, 'tp', axis=0, tiled=True)  42.4 us
    all_gather x1, waiting for transfers between devices, body(): shard_rows = lax.all_gather(expert_normed, 'tp', axis=0, tiled=True)  19.8 us
    dot_general x1, matrix products, body(): jnp.einsum('sepf,efd->sepd', inner, w_drop, preferred_element_type=jnp.fl...  10.5 us
    reduce_scatter x1, waiting for transfers between devices, body(): lax.psum_scatter(jnp.dot(head_rows, w_output, preferred_element_type=jnp....  10.2 us
    gather x1, local copies, waits for them, and re-layouts, body(): returned.reshape(experts * capacity, -1)[slot_index]  7.94 us
    all_to_all x1, starting transfers between devices, body(): lax.all_to_all(outgoing, ('ep', 'tp'), split_axis=0, concat_axis=0, tiled...  7.58 us
    add x8, other arithmetic, advance(): return (jnp.exp(decay_sum)[:, :, None] * state + addition, state)  7.47 us
  transfers between devices with their start and end apart: 6, of which 3 were waited for; matrix products, arithmetic and copies ran while one was open for 31% of the time, Pallas kernels for 0%

commit v1 on v0

--- a/solution.py
+++ b/solution.py
@@ -2,6 +2,7 @@
 import jax.numpy as jnp
 from jax import lax
 from jax.sharding import PartitionSpec as P
+from jax.lax import axis_index, axis_size, ppermute
 
 DK = 64
 DV = 128
@@ -9,6 +10,22 @@
 epsilon = 1e-05
 gate_norm = 16.0
 highest = lax.Precision.HIGHEST
+
+
+def obtain_chunk(x0):
+    n_chips = axis_size("tp")
+    now = sorted(((num, (num + 1) % n_chips) for num in range(n_chips)))
+    current_arr = x0
+    frames = [current_arr]
+    w = 1
+    while w < n_chips:
+        current_arr = ppermute(current_arr, "tp", now)
+        frames.insert(0, current_arr)
+        w += 1
+    left_arr = jnp.concatenate(frames, axis=0)
+    low = axis_index("tp")
+    carry_in = low + 1
+    return jnp.roll(left_arr, shift=carry_in * x0.shape[0], axis=0)
 
 
 def entering_2(value, axis, combine, identity):
@@ -161,7 +178,7 @@
         tiled=True,
     )
     expert_normed = layer_norm(expert_rows, ffn_gain)
-    shard_rows = lax.all_gather(expert_normed, "tp", axis=0, tiled=True)
+    shard_rows = obtain_chunk(expert_normed)
     hidden = (
         jax.nn.silu(jnp.dot(shard_rows, shared_gate, preferred_element_type=jnp.float32))
         * jnp.dot(shard_rows, shared_lift, preferred_element_type=jnp.float32)

time: 299 us -> 313 us (1.047)
  local copies, waits for them, and re-layouts: 33.6 us -> 41.9 us
  waiting for transfers between devices: 73.2 us -> 79.3 us
    ppermute x0 -> x3, waiting for transfers between devices: none -> 51.1 us  [obtain_chunk(): current_arr = ppermute(current_arr, 'tp', now)]
    all_gather x1, waiting for transfers between devices: 42.4 us -> 17.1 us  [body(): shard_rows = lax.all_gather(mix_normed, 'tp', axis=0, tiled=True)]
    all_gather x1 -> x0, waiting for transfers between devices: 19.8 us -> none  [body(): shard_rows = lax.all_gather(expert_normed, 'tp', axis=0, tiled=True)]
    unnamed x28 -> x42, local copies, waits for them, and re-layouts: 2.16 us -> 11.2 us
  transfers between devices with their start and end apart: 6 -> 8, of which waited for: 3 -> 5; matrix products, arithmetic and copies ran while one was open for 31% -> 32% of each run, Pallas kernels for 0% -> 0%
where the time goes in v1:
time: 313 us; the launch traced here: 311 us
  blocking collectives  86.5 us (28%)
  waiting for transfers between devices  79.3 us (25%)
  matrix products  44 us (14%)
  local copies, waits for them, and re-layouts  41.9 us (13%)
  other arithmetic  32.4 us (10%)
  between operations  14.3 us (5%)
  starting transfers between devices  12.6 us (4%)
    all_gather x2, blocking collectives, entering_2(): lax.all_gather(part.astype(kind), axis)  86.5 us
    ppermute x3, waiting for transfers between devices, obtain_chunk(): current_arr = ppermute(current_arr, 'tp', now)  51.1 us
    all_gather x1, waiting for transfers between devices, body(): shard_rows = lax.all_gather(mix_normed, 'tp', axis=0, tiled=True)  17.1 us
    unnamed x42, local copies, waits for them, and re-layouts  11.2 us
    reduce_scatter x1, waiting for transfers between devices, body(): lax.psum_scatter(jnp.dot(head_rows, w_output, preferred_element_type=jnp....  11 us
    dot_general x1, matrix products, body(): jnp.einsum('sepf,efd->sepd', inner, w_drop, preferred_element_type=jnp.fl...  10.1 us
    gather x1, local copies, waits for them, and re-layouts, body(): returned.reshape(experts * capacity, -1)[slot_index]  7.95 us
    all_to_all x1, starting transfers between devices, body(): lax.all_to_all(outgoing, ('ep', 'tp'), split_axis=0, concat_axis=0, tiled...  7.58 us
  transfers between devices with their start and end apart: 8, of which 5 were waited for; matrix products, arithmetic and copies ran while one was open for 32% of the time, Pallas kernels for 0%

profile of v1, /device:TPU:0, one launch (start us, length us, event | category | flops | bytes accessed | tf_op | source)
XLA Modules:
  0.0 311.2 jit_solution(9350790342577338965)
XLA Ops:
  10.2 1.3 fusion.26
  13.3 2.4 scatter_custom_fusion
  15.8 1.4 fusion.28
  18.1 6.0 %gather_fusion = bf16[1024,2048]{1,0:T(8,128)(2,1)} fusion(bf16[129,2048]{1,0:T(8,128)(2,1)S(1)} %concatenate.10, s32[1024]{0:T(1024)S(1)} %fusion.56), kind=kCustom, calls=%fused_computation | custom fusion | bytes 8392704 | tf_op jit(solution)/shard_map/gather | solution.py:209
  24.1 7.6 %all-to-all-start = ((bf16[16,64,2048]{2,1,0:T(8,128)(2,1)}), bf16[16,64,2048]{2,1,0:T(8,128)(2,1)}, u32[]{:S(2)}, u32[]{:S(2)}) async-start(bf16[16,64,2048]{2,1,0:T(8,128)(2,1)} %bitcast.140), calls=%async_computation.2 | async-start | bytes 8388608 | tf_op jit(solution)/shard_map/all_to_all | solution.py:210
  32.3 31.5 %collective-permute-done = bf16[128,2048]{1,0:T(8,128)(2,1)S(1)} collective-permute-done((bf16[128,2048]{1,0:T(8,128)(2,1)}, bf16[128,2048]{1,0:T(8,128)(2,1)S(1)}, u32[]{:S(2)}, u32[]{:S(2)}) %collective-permute-start) | collective-permute-done | bytes 524320 | tf_op jit(solution)/shard_map/ppermute | solution.py:22
  64.9 12.8 %collective-permute-done.1 = bf16[128,2048]{1,0:T(8,128)(2,1)} collective-permute-done((bf16[128,2048]{1,0:T(8,128)(2,1)S(1)}, bf16[128,2048]{1,0:T(8,128)(2,1)}, u32[]{:S(2)}, u32[]{:S(2)}) %collective-permute-start.1) | collective-permute-done | bytes 524320 | tf_op jit(solution)/shard_map/ppermute | solution.py:22
  80.0 6.8 %collective-permute-done.2 = bf16[128,2048]{1,0:T(8,128)(2,1)} collective-permute-done((bf16[128,2048]{1,0:T(8,128)(2,1)}, bf16[128,2048]{1,0:T(8,128)(2,1)}, u32[]{:S(2)}, u32[]{:S(2)}) %collective-permute-start.2) | collective-permute-done | bytes 524320 | tf_op jit(solution)/shard_map/ppermute | solution.py:22
  94.1 2.0 copy-done.2
  96.8 5.6 %convolution_convert_fusion.1 = bf16[512,2048]{1,0:T(8,128)(2,1)} fusion(bf16[128,2048]{1,0:T(8,128)(2,1)} %param.45, f32[512,128]{1,0:T(8,128)S(1)} %fusion.10, bf16[2048,128]{1,0:T(8,128)(2,1)} %param.43, bf16[1024,2048]{1,0:T(8,128)(2,1)} %copy-done.2, s32[]{:T(128)S(6)} %select_n.73), kind=kOutput, calls=%fused_computation.12 | convolution fusion | flops 538312704 | bytes 5505028 | tf_op jit(solution)/shard_map/dot_general | solution.py:187
  102.4 17.1 %all-gather.5.cloned.1.call-done = bf16[512,2048]{1,0:T(8,128)(2,1)} async-done(((bf16[128,2048]{1,0:T(8,128)(2,1)}), bf16[512,2048]{1,0:T(8,128)(2,1)}) %all-gather.5.cloned.1.call-update) | async-done | bytes 2097168 | tf_op jit(solution)/shard_map/all_gather | solution.py:133
  119.6 2.7 fusion.41
  123.2 2.6 convolution_convert_fusion.5
  126.9 2.6 convolution_convert_fusion.4
  130.6 2.6 convolution_convert_fusion.3
  133.3 3.1 exponential_multiply_fusion
  136.4 1.4 fusion.34
  137.8 6.6 %fusion.3 = f32[16,64,512]{2,1,0:T(8,128)} fusion(bf16[16,64,2048]{2,1,0:T(8,128)(2,1)} %all-to-all-done, bf16[1,2048,512]{2,1,0:T(8,128)(2,1)} %param.41), kind=kOutput, calls=%fused_computation.17 | convolution fusion | flops 2147483648 | bytes 8388608 | tf_op jit(solution)/shard_map/sepd,edf->sepf/dot_general | solution.py:214
  144.4 10.1 %convolution_convert_fusion = bf16[16,64,2048]{2,1,0:T(8,128)(2,1)} fusion(bf16[1,512,2048]{2,1,0:T(8,128)(2,1)S(1)} %copy-done, f32[16,64,512]{2,1,0:T(8,128)} %fusion.3, bf16[16,64,2048]{2,1,0:T(8,128)(2,1)} %all-to-all-done, bf16[1,2048,512]{2,1,0:T(8,128)(2,1)} %param.40), kind=kOutput, calls=%fused_computation.11 | convolution fusion | flops 4300210176 | bytes 14680064 | tf_op jit(solution)/shard_map/sepf,efd->sepd/dot_general | solution.py:216
  154.5 4.5 %all-to-all-start.1 = ((bf16[16,64,2048]{2,1,0:T(8,128)(2,1)}), bf16[16,64,2048]{2,1,0:T(8,128)(2,1)}, u32[]{:S(2)}, u32[]{:S(2)}) async-start(bf16[16,64,2048]{2,1,0:T(8,128)(2,1)} %convolution_convert_fusion), calls=%async_computation.3 | async-start | bytes 8388608 | tf_op jit(solution)/shard_map/all_to_all | solution.py:217
  159.1 12.8 %while.27 = (s32[]{:T(128)}, f32[2,64,128]{2,1,0:T(8,128)S(1)}, f32[8,2,64,128]{3,2,1,0:T(8,128)}, f32[8,2,64]{2,0,1:T(8,128)S(1)}, f32[8,2,64,128]{3,2,1,0:T(8,128)}, /*index=5*/s32[]{:T(128)}, s32[]{:T(128)}) while((s32[]{:T(128)}, f32[2,64,128]{2,1,0:T(8,128)S(1)}, f32[8,2,64,128]{3,2,1,0:T(8,128)}, f32[8,2,64]{2,0,1:T(8,128)S(1)}, ...), condition=%wide.region_4.5_spmd.clone, body=%wide.region_3.4_spmd.clone.sunk | while | flops 65539 | bytes 330848 | solution.py:91
  172.7 2.1 convolution_select_fusion
  175.3 1.7 fusion.23
  181.4 52.0 %all-gather.2 = bf16[4,2,64]{2,1,0:T(2,128)(2,1)S(1)} all-gather(bf16[1,2,64]{2,1,0:T(2,128)(2,1)S(1)} %bitcast.150), channel_id=2, replica_groups=mesh['grp'=2,'ep'=4,'tp'=4] {'ep'}, dimensions={0}, use_global_device_ids=true | all-gather | bytes 1280 | tf_op jit(solution)/shard_map/all_gather | solution.py:34
  233.3 34.5 %all-gather.1 = bf16[8,64,128]{2,1,0:T(8,128)(2,1)S(1)} all-gather(bf16[2,64,128]{2,1,0:T(8,128)(2,1)S(1)} %convert_element_type.114), channel_id=3, replica_groups=mesh['grp'=2,'ep'=4,'tp'=4] {'ep'}, dimensions={0}, use_global_device_ids=true | all-gather | bytes 163840 | tf_op jit(solution)/shard_map/all_gather | solution.py:34
  268.4 1.6 multiply_reduce_fusion.1
  270.1 3.4 %convolution_convert_fusion.2 = bf16[512,2048]{1,0:T(8,128)(2,1)} fusion(bf16[512,256]{0,1:T(8,128)(2,1)S(1)} %bitcast.142, bf16[256,2048]{1,0:T(8,128)(2,1)} %param.37), kind=kOutput, calls=%fused_computation.13 | convolution fusion | flops 537919488 | bytes 3407872 | tf_op jit(solution)/shard_map/dot_general | solution.py:175
  273.7 8.0 %gather_fusion.1 = bf16[512,2048]{1,0:T(8,128)(2,1)} fusion(bf16[1024,2048]{1,0:T(8,128)(2,1)} %bitcast.29, s32[1024]{0:T(1024)S(1)} %pad_clamp_fusion), kind=kCustom, calls=%fused_computation.1 | custom fusion | bytes 4196352 | tf_op jit(solution)/shard_map/gather | solution.py:224
  281.6 4.8 %reshape.187 = f32[128,4,2048]{2,1,0:T(4,128)} reshape(bf16[512,2048]{1,0:T(8,128)(2,1)} %gather_fusion.1) | data formatting | bytes 6291456 | tf_op jit(solution)/shard_map/convert_element_type | solution.py:227
  286.4 5.4 %multiply_reduce_fusion = f32[128,2048]{1,0:T(8,128)S(1)} fusion(f32[128,4,2048]{2,1,0:T(4,128)} %reshape.187, f32[128,4]{1,0:T(8,128)S(1)} %copy.70), kind=kLoop, calls=%fused_computation.10 | loop fusion | flops 1835008 | bytes 5244928 | tf_op jit(solution)/shard_map/reduce_sum | solution.py:227
  291.8 1.9 add_convert_fusion
  293.7 11.0 %reduce-scatter.3.cloned.1.call-done = bf16[128,2048]{1,0:T(8,128)(2,1)} async-done(((bf16[512,2048]{1,0:T(8,128)(2,1)}), bf16[128,2048]{1,0:T(8,128)(2,1)}) %reduce-scatter.3.cloned.1.call-update) | async-done | bytes 524304 | tf_op jit(solution)/shard_map/reduce_scatter | solution.py:174
  (146 shorter events, 40.3 us)
Async XLA Ops:
  7.2 137.2 %copy-start = (bf16[1,512,2048]{2,1,0:T(8,128)(2,1)S(1)}, bf16[1,512,2048]{2,1,0:T(8,128)(2,1)}, u32[]{:S(2)}) copy-start(bf16[1,512,2048]{2,1,0:T(8,128)(2,1)} %param.42) | copy-start | bytes 6291460
  13.3 2.5 copy-start.11
  17.2 0.8 copy-start.7
  24.1 8.1 %copy-start.3 = (bf16[128,2048]{1,0:T(8,128)(2,1)S(1)}, bf16[128,2048]{1,0:T(8,128)(2,1)}, u32[]{:S(2)}) copy-start(bf16[128,2048]{1,0:T(8,128)(2,1)} %param.25) | copy-start | bytes 1572868
  24.1 53.6 %copy-start.10 = (f32[2048]{0:T(1024)S(1)}, f32[2048]{0:T(1024)}, u32[]{:S(2)}) copy-start(f32[2048]{0:T(1024)} %param.27) | copy-start | bytes 24580
  24.1 54.9 %copy-start.13 = (f32[2,512]{1,0:T(2,128)S(1)}, f32[2,512]{1,0:T(2,128)}, u32[]{:S(2)}) copy-start(f32[2,512]{1,0:T(2,128)} %param.35) | copy-start | bytes 12292
  24.1 113.7 %all-to-all-start = ((bf16[16,64,2048]{2,1,0:T(8,128)(2,1)}), bf16[16,64,2048]{2,1,0:T(8,128)(2,1)}, u32[]{:S(2)}, u32[]{:S(2)}) async-start(bf16[16,64,2048]{2,1,0:T(8,128)(2,1)} %bitcast.140), calls=%async_computation.2 | async-start | bytes 8388608 | tf_op jit(solution)/shard_map/all_to_all | solution.py:210
  31.7 58.4 %copy-start.1 = (bf16[128,2048]{1,0:T(8,128)(2,1)S(1)}, bf16[128,2048]{1,0:T(8,128)(2,1)}, u32[]{:S(2)}) copy-start(bf16[128,2048]{1,0:T(8,128)(2,1)} %param.26) | copy-start | bytes 1572868
  31.7 58.4 %copy-start.9 = (f32[2048]{0:T(1024)S(1)}, f32[2048]{0:T(1024)}, u32[]{:S(2)}) copy-start(f32[2048]{0:T(1024)} %param.28) | copy-start | bytes 24580
  31.7 87.8 %all-gather.5.cloned.1.call-start = ((), (), s32[]{:S(2)}) async-start(), calls=%async_computation.4 | async-start | bytes 2621440 | tf_op jit(solution)/shard_map/all_gather | solution.py:133
  31.8 32.1 %collective-permute-start = (bf16[128,2048]{1,0:T(8,128)(2,1)}, bf16[128,2048]{1,0:T(8,128)(2,1)S(1)}, u32[]{:S(2)}, u32[]{:S(2)}) collective-permute-start(bf16[128,2048]{1,0:T(8,128)(2,1)} %copy-done.7), channel_id=1, source_target_pairs={{0,1},{1,2},{2,3},{3,0},{4,5},{5,6},{6,7},{7,4},{8,9},{9,10},{10,1... | collective-permute-start | bytes 1572872 | tf_op jit(solution)/shard_map/ppermute | solution.py:22
  63.8 0.8 copy-start.6
  64.6 13.1 %collective-permute-start.1 = (bf16[128,2048]{1,0:T(8,128)(2,1)S(1)}, bf16[128,2048]{1,0:T(8,128)(2,1)}, u32[]{:S(2)}, u32[]{:S(2)}) collective-permute-start(bf16[128,2048]{1,0:T(8,128)(2,1)S(1)} %collective-permute-done), channel_id=1, source_target_pairs={{0,1},{1,2},{2,3},{3,0},{4,5},{5,6},{6,7},{7,4},{8,9},{9,10},{10,1... | collective-permute-start | bytes 1572872 | tf_op jit(solution)/shard_map/ppermute | solution.py:22
  77.7 9.1 %collective-permute-start.2 = (bf16[128,2048]{1,0:T(8,128)(2,1)}, bf16[128,2048]{1,0:T(8,128)(2,1)}, u32[]{:S(2)}, u32[]{:S(2)}) collective-permute-start(bf16[128,2048]{1,0:T(8,128)(2,1)} %collective-permute-done.1), channel_id=1, source_target_pairs={{0,1},{1,2},{2,3},{3,0},{4,5},{5,6},{6,7},{7,4},{8,9},{9,10},{10,1... | collective-permute-start | bytes 1572872 | tf_op jit(solution)/shard_map/ppermute | solution.py:22
  78.9 212.9 %reduce-scatter.5.cloned.1.call-start = ((), (), s32[]{:S(2)}) async-start(), calls=%async_computation.6 | async-start | bytes 2621440 | tf_op jit(solution)/shard_map/reduce_scatter | solution.py:186
  80.0 16.2 %copy-start.8 = (bf16[2048,128]{1,0:T(8,128)(2,1)S(1)}, bf16[2048,128]{1,0:T(8,128)(2,1)}, u32[]{:S(2)}) copy-start(bf16[2048,128]{1,0:T(8,128)(2,1)} %param.44) | copy-start | bytes 1572868
  94.1 2.0 copy-start.2
  96.8 22.7 %copy-start.16 = (bf16[2048,32]{0,1:T(8,128)(2,1)S(1)}, bf16[2048,32]{0,1:T(8,128)(2,1)}, u32[]{:S(2)}) copy-start(bf16[2048,32]{0,1:T(8,128)(2,1)} %param.32) | copy-start | bytes 393220
  123.2 10.2 %copy-start.4 = (f32[8,64,2,64]{3,0,1,2:T(8,128)}, f32[8,64,2,64]{3,0,1,2:T(8,128)S(1)}, u32[]{:S(2)}) copy-start(f32[8,64,2,64]{3,0,1,2:T(8,128)S(1)} %fusion.37) | copy-start | bytes 786436
  154.5 119.2 %all-to-all-start.1 = ((bf16[16,64,2048]{2,1,0:T(8,128)(2,1)}), bf16[16,64,2048]{2,1,0:T(8,128)(2,1)}, u32[]{:S(2)}, u32[]{:S(2)}) async-start(bf16[16,64,2048]{2,1,0:T(8,128)(2,1)} %convolution_convert_fusion), calls=%async_computation.3 | async-start | bytes 8388608 | tf_op jit(solution)/shard_map/all_to_all | solution.py:217
  159.0 145.7 %reduce-scatter.3.cloned.1.call-start = ((), (), s32[]{:S(2)}) async-start(), calls=%async_computation.5 | async-start | bytes 2621440 | tf_op jit(solution)/shard_map/reduce_scatter | solution.py:174
  175.3 3.9 %copy-start.5 = (f32[8,64,2,64]{3,0,1,2:T(8,128)S(1)}, f32[8,64,2,64]{3,0,1,2:T(8,128)}, u32[]{:S(2)}) copy-start(f32[8,64,2,64]{3,0,1,2:T(8,128)} %get-tuple-element.200) | copy-start | bytes 786436
  175.3 94.8 %copy-start.15 = (f32[128]{0:T(128)S(1)}, f32[128]{0:T(128)}, u32[]{:S(2)}) copy-start(f32[128]{0:T(128)} %param.36) | copy-start | bytes 1540
  268.4 5.2 %copy-start.14 = (f32[128,4]{0,1:T(4,128)S(1)}, f32[128,4]{0,1:T(4,128)}, u32[]{:S(2)}) copy-start(f32[128,4]{0,1:T(4,128)} %param.39) | copy-start | bytes 6148
  268.4 5.3 %copy-start.12 = (s32[512,1]{0,1:T(1,128)S(1)}, s32[512,1]{0,1:T(1,128)}, u32[]{:S(2)}) copy-start(s32[512,1]{0,1:T(1,128)} %copy-done.11) | copy-start | bytes 6148
Sparse Core Ops, SparseCore 0:
  79.0 40.5 all-gather.4
  122.1 30.2 reduce-scatter.4
  273.7 30.9 reduce-scatter.2
